TPU v7x, 32 devices: a whole 2x2x4 slice. The times are simulated.
32 devices in a mesh: sp: 8 (over z, y), dp: 4 (over x, core).
Axes of the slice: x: 2, y: 2, z: 4, core: 2. Of those that a mesh axis runs over, the one named last changes fastest.
Arguments:
- queries: bfloat16 [4096, 6144], P(('dp', 'sp')), may hold values from -360 to 360
- latent: bfloat16 [4096, 1024], P(('dp', 'sp')), may hold values from -6 to 6
- rope_key: bfloat16 [4096, 64], P(('dp', 'sp')), may hold values from -6 to 6
- latent_gain: float32 [1024], replicated, may hold values from 0.1 to 1.9
- kv_weight: bfloat16 [1024, 8192], P(None, 'dp'), may hold values from -0.1875 to 0.1875
- gate: bfloat16 [4096, 4096], P(('dp', 'sp')), may hold values from -6 to 6
- out_gain: float32 [4096], replicated, may hold values from 0.1 to 1.9
Outputs:
- attended: bfloat16 [4096, 4096], P(('dp', 'sp'))
All inputs are finite; a program needn't handle non-finite values.
Results may differ from a plain program's by a relative error of at most 0.007.
Values may be sent and summed in bfloat16 or wider, within the bound.
A program may use at most 128 MiB of HBM per device.

v0:
```python
import jax
import jax.numpy as jnp
from jax import lax
from jax.sharding import PartitionSpec as P

HEADS = 32
NOPE = 128
ROPE = 64
VDIM = 128


EPS = 1e-06
THETA = 10000.0


def rotary(values, position):
    half_width = values.shape[-1] // 2
    inverse = THETA ** (-jnp.arange(half_width, dtype=jnp.float32) / half_width)
    angles = position.astype(jnp.float32)[:, None] * inverse[None, :]
    if values.ndim == 3:
        angles = angles[:, None, :]
    cosine = jnp.cos(angles)
    sine_part = jnp.sin(angles)
    front_half = values[..., :half_width].astype(jnp.float32)
    back_half = values[..., half_width:].astype(jnp.float32)
    turned = jnp.concatenate(
        [front_half * cosine - back_half * sine_part, back_half * cosine + front_half * sine_part],
        axis=-1,
    )
    return turned.astype(jnp.bfloat16)


def attend(query_block, keys_plain, keys_rotated, values):
    scores = jnp.einsum(
        "qhd,khd->hqk", query_block[..., :NOPE], keys_plain, preferred_element_type=jnp.float32
    )
    scores = scores + jnp.einsum(
        "qhr,kr->hqk", query_block[..., NOPE:], keys_rotated, preferred_element_type=jnp.float32
    )
    scores = scores * (NOPE + ROPE) ** (-0.5)
    row_max = jnp.max(scores, axis=-1, keepdims=True)
    raised = jnp.exp(scores - row_max)
    weights = (raised / jnp.sum(raised, axis=-1, keepdims=True)).astype(jnp.bfloat16)
    result = jnp.einsum("hqk,khd->qhd", weights, values, preferred_element_type=jnp.float32)
    return result.astype(jnp.bfloat16)


def per_device(queries, latent, rope_key, latent_gain, kv_weight, gate, out_gain):
    own_tokens = queries.shape[0]
    groups = lax.axis_size("sp")
    seq_len = own_tokens * groups
    offset = lax.axis_index("sp") * own_tokens
    position = offset + jnp.arange(own_tokens, dtype=jnp.int32)
    widened = latent.astype(jnp.float32)
    normed = (
        widened * lax.rsqrt(jnp.mean(widened * widened, axis=-1, keepdims=True) + EPS) * latent_gain
    ).astype(jnp.bfloat16)
    shard_columns = jnp.dot(
        lax.all_gather(normed, "dp", axis=0, tiled=True),
        kv_weight,
        preferred_element_type=jnp.float32,
    ).astype(jnp.bfloat16)
    keyval = lax.all_to_all(shard_columns, "dp", split_axis=0, concat_axis=1, tiled=True)
    head_queries = queries.reshape(own_tokens, HEADS, NOPE + ROPE)
    head_queries = jnp.concatenate(
        [head_queries[..., :NOPE], rotary(head_queries[..., NOPE:], position)], axis=-1
    )
    head_queries = head_queries.reshape(own_tokens, HEADS * (NOPE + ROPE))
    rotated_all = lax.all_gather(rotary(rope_key, position), "sp", axis=0, tiled=True)
    query_all, kv_all = (
        lax.all_to_all(head_queries, "sp", split_axis=1, concat_axis=0, tiled=True),
        lax.all_to_all(keyval, "sp", split_axis=1, concat_axis=0, tiled=True),
    )
    local_heads = HEADS // groups
    rows_all = query_all.shape[0]
    seq_count = rows_all // seq_len
    block_rows = min(512, seq_len)
    block_count = seq_len // block_rows

    def one_sequence(operands):
        query_seq, kv_seq, rope_seq = operands
        keys_plain = kv_seq[..., :NOPE]
        values = kv_seq[..., NOPE:]
        blocks = query_seq.reshape(block_count, block_rows, local_heads, NOPE + ROPE)
        result = lax.map(
            lambda piece_rows: attend(piece_rows, keys_plain, rope_seq, values), blocks
        )
        return result.reshape(seq_len, local_heads * VDIM)

    heads_out = lax.map(
        one_sequence,
        (
            query_all.reshape(seq_count, seq_len, local_heads, NOPE + ROPE),
            kv_all.reshape(seq_count, seq_len, local_heads, NOPE + VDIM),
            rotated_all.reshape(seq_count, seq_len, ROPE),
        ),
    )
    heads_out = heads_out.reshape(rows_all, local_heads * VDIM)
    token_rows = lax.all_to_all(heads_out, "sp", split_axis=0, concat_axis=1, tiled=True)
    gated_rows = token_rows.astype(jnp.float32) * jax.nn.silu(gate.astype(jnp.float32))
    scale_rows = lax.rsqrt(jnp.mean(gated_rows * gated_rows, axis=-1, keepdims=True) + EPS)
    return (gated_rows * scale_rows * out_gain).astype(jnp.bfloat16)


def solution(mesh):
    return jax.shard_map(
        per_device,
        mesh=mesh,
        in_specs=(
            P(("dp", "sp"), None),
            P(("dp", "sp"), None),
            P(("dp", "sp"), None),
            P(),
            P(None, "dp"),
            P(("dp", "sp"), None),
            P(),
        ),
        out_specs=P(("dp", "sp"), None),
        check_vma=False,
    )
```

profile of v0, /device:TPU:0, one launch (start us, length us, event | category | flops | bytes accessed | tf_op | source)
XLA Modules:
  0.0 260.2 jit_solution(7469383440938197503)
XLA Ops:
  6.6 1.9 copy.21
  8.9 1.3 pad_maximum_fusion
  10.2 7.4 %all-to-all-start = ((bf16[128,8,768]{0,2,1:T(8,128)(2,1)}), bf16[128,8,768]{0,2,1:T(8,128)(2,1)}, u32[]{:S(2)}, u32[]{:S(2)}) async-start(bf16[128,8,768]{0,2,1:T(8,128)(2,1)} %bitcast.6), calls=%async_computation | async-start | bytes 3145728 | tf_op jit(solution)/shard_map/all_to_all | solution.py:71
  18.7 19.4 %all-gather.2.cloned.1.call-done = bf16[512,1024]{1,0:T(8,128)(2,1)} async-done(((bf16[128,1024]{1,0:T(8,128)(2,1)}), bf16[512,1024]{1,0:T(8,128)(2,1)}) %all-gather.2.cloned.1.call-update) | async-done | bytes 1048592 | tf_op jit(solution)/shard_map/all_gather | solution.py:59
  38.2 6.2 %convolution_convert_fusion = bf16[512,2048]{1,0:T(8,128)(2,1)} fusion(bf16[512,1024]{1,0:T(8,128)(2,1)} %all-gather.2.cloned.1.call-done, bf16[1024,2048]{1,0:T(8,128)(2,1)} %param.13), kind=kOutput, calls=%fused_computation.15 | convolution fusion | flops 2148532224 | bytes 7340032 | tf_op jit(solution)/shard_map/dot_general | solution.py:58
  44.3 3.0 %copy.23 = bf16[4,128,2048]{1,2,0:T(8,128)(2,1)S(1)} copy(bf16[4,128,2048]{2,1,0:T(8,128)(2,1)} %bitcast.57) | data formatting | bytes 4194304 | tf_op jit(solution)/shard_map/all_to_all | solution.py:63
  47.4 7.4 %all-to-all-done = bf16[128,8,768]{0,2,1:T(8,128)(2,1)} async-done(((bf16[128,8,768]{0,2,1:T(8,128)(2,1)}), bf16[128,8,768]{0,2,1:T(8,128)(2,1)}, u32[]{:S(2)}, u32[]{:S(2)}) %all-to-all-start) | async-done | bytes 1572896 | tf_op jit(solution)/shard_map/all_to_all | solution.py:71
  54.8 28.9 %all_to_all.61 = bf16[4,128,2048]{1,2,0:T(8,128)(2,1)} all-to-all(bf16[4,128,2048]{1,2,0:T(8,128)(2,1)S(1)} %copy.23), channel_id=1, replica_groups=mesh['sp'=8,'dp'=4] {'dp'}, dimensions={0} | all-to-all | bytes 4194304 | tf_op jit(solution)/shard_map/all_to_all | solution.py:63
  83.7 4.3 %all-to-all-start.2 = ((bf16[128,8,1024]{0,2,1:T(8,128)(2,1)}), bf16[128,8,1024]{0,2,1:T(8,128)(2,1)}, u32[]{:S(2)}, u32[]{:S(2)}) async-start(bf16[128,8,1024]{0,2,1:T(8,128)(2,1)} %bitcast.10), calls=%async_computation.2 | async-start | bytes 4194304 | tf_op jit(solution)/shard_map/all_to_all | solution.py:72
  88.0 67.0 %all_gather.7 = bf16[1024,64]{0,1:T(8,128)(2,1)S(1)} all-gather(bf16[128,64]{0,1:T(8,128)(2,1)S(1)} %pad_maximum_fusion.1), channel_id=1, replica_groups=mesh['sp'=8,'dp'=4] {'sp'}, dimensions={0}, use_global_device_ids=true | all-gather | bytes 147456 | tf_op jit(solution)/shard_map/all_gather | solution.py:69
  155.0 2.4 copy.22
  157.4 2.2 reshape.121
  159.6 4.6 %copy.25 = bf16[2,512,4,192]{3,1,2,0:T(8,128)(2,1)S(1)} copy(bf16[2,512,4,192]{1,0,3,2:T(2,128)(2,1)} %reshape.121) | data formatting | bytes 3145728 | tf_op jit(solution)/shard_map/while/body/eval_jaxpr/while | solution.py:85
  164.2 4.3 %copy.24 = bf16[8,128,1024]{1,0,2:T(8,128)(2,1)} copy(bf16[8,128,1024]{1,2,0:T(8,128)(2,1)} %bitcast.11) | data formatting | bytes 4194304 | tf_op jit(solution)/shard_map/all_to_all | solution.py:72
  168.5 4.1 %squeeze.15 = bf16[1024,4,256]{0,2,1:T(8,128)(2,1)} reshape(bf16[8,128,1024]{1,0,2:T(8,128)(2,1)} %copy.24) | data formatting | bytes 4194304 | tf_op jit(solution)/shard_map/while/body/jit(dynamic_index_in_dim)/squeeze | solution.py:90
  172.6 3.0 %fusion.26 = (bf16[1024,4,128]{0,2,1:T(8,128)(2,1)}, bf16[1024,4,128]{0,2,1:T(8,128)(2,1)}) fusion(bf16[1024,4,256]{0,2,1:T(8,128)(2,1)} %squeeze.15), kind=kLoop, calls=%fused_computation.55 | loop fusion | bytes 4194304 | tf_op jit(solution)/shard_map/while/body/eval_jaxpr/slice | solution.py:83
  175.7 1.6 copy.26
  177.3 2.3 copy.27
  179.6 37.9 %while.17 = (s32[]{:T(128)}, bf16[2,512,4,128]{3,2,1,0:T(4,128)(2,1)}, bf16[2,512,4,192]{3,1,2,0:T(8,128)(2,1)S(1)}, bf16[1024,4,128]{2,0,1:T(8,128)(2,1)S(1)}, ...) while((s32[]{:T(128)}, bf16[2,512,4,128]{3,2,1,0:T(4,128)(2,1)}, ...), condition=%wide.region_4.5_spmd, body=%wide.region_1.4_spmd.sunk | while | flops 1357123584 | bytes 81937008 | solution.py:85
  182.2 2.0 fusion.53
  185.4 10.9 %fusion.54 = bf16[1,512,4,128]{3,1,2,0:T(8,128)(2,1)} fusion(bf16[1024,4,128]{2,0,1:T(8,128)(2,1)} %get-tuple-element.141, f32[4,512]{1,0:T(4,128)S(1)} %fusion.53, f32[4,512,1024]{2,1,0:T(8,128)} %copy-done), kind=kOutput, calls=%fused_computation.7.clone.1 | convolution fusion | flops 543427584 | bytes 9969664 | tf_op jit(solution)/shard_map/while/body/eval_jaxpr/while/body/eval_jaxpr/hqk,khd->qhd/dot_general | solution.py:44
  196.3 2.2 copy_dynamic-update-slice_fusion.2
  201.1 2.0 fusion.53
  204.3 10.9 %fusion.54 = bf16[1,512,4,128]{3,1,2,0:T(8,128)(2,1)} fusion(bf16[1024,4,128]{2,0,1:T(8,128)(2,1)} %get-tuple-element.141, f32[4,512]{1,0:T(4,128)S(1)} %fusion.53, f32[4,512,1024]{2,1,0:T(8,128)} %copy-done), kind=kOutput, calls=%fused_computation.7.clone.1 | convolution fusion | flops 543427584 | bytes 9969664 | tf_op jit(solution)/shard_map/while/body/eval_jaxpr/while/body/eval_jaxpr/hqk,khd->qhd/dot_general | solution.py:44
  215.3 2.2 copy_dynamic-update-slice_fusion.2
  217.5 2.3 all_to_all.55
  219.8 3.6 %all-to-all-start.3 = ((bf16[8,128,512]{2,1,0:T(8,128)(2,1)}), bf16[8,128,512]{2,1,0:T(8,128)(2,1)S(1)}, u32[]{:S(2)}, u32[]{:S(2)}) async-start(bf16[8,128,512]{2,1,0:T(8,128)(2,1)} %all_to_all.55), calls=%async_computation.3 | async-start | bytes 2097152 | tf_op jit(solution)/shard_map/all_to_all | solution.py:99
  224.1 21.0 %all-to-all-done.3 = bf16[8,128,512]{2,1,0:T(8,128)(2,1)S(1)} async-done(((bf16[8,128,512]{2,1,0:T(8,128)(2,1)}), bf16[8,128,512]{2,1,0:T(8,128)(2,1)S(1)}, u32[]{:S(2)}, u32[]{:S(2)}) %all-to-all-start.3) | async-done | bytes 1048608 | tf_op jit(solution)/shard_map/all_to_all | solution.py:99
  245.1 1.6 convert_bitcast_fusion
  246.7 1.9 copy.29
  249.4 1.7 multiply_convert_fusion
  251.1 2.3 copy.31
  (36 shorter events, 10.3 us)
Async XLA Ops:
  6.5 2.0 copy-start.4
  10.2 7.5 %copy-start.1 = (bf16[128,1024]{1,0:T(8,128)(2,1)S(1)}, bf16[128,1024]{1,0:T(8,128)(2,1)}, u32[]{:S(2)}) copy-start(bf16[128,1024]{1,0:T(8,128)(2,1)} %param.10) | copy-start | bytes 786436
  10.2 7.6 %copy-start.5 = (f32[1024]{0:T(1024)S(1)}, f32[1024]{0:T(1024)}, u32[]{:S(2)}) copy-start(f32[1024]{0:T(1024)} %param.12) | copy-start | bytes 12292
  10.2 44.5 %all-to-all-start = ((bf16[128,8,768]{0,2,1:T(8,128)(2,1)}), bf16[128,8,768]{0,2,1:T(8,128)(2,1)}, u32[]{:S(2)}, u32[]{:S(2)}) async-start(bf16[128,8,768]{0,2,1:T(8,128)(2,1)} %bitcast.6), calls=%async_computation | async-start | bytes 3145728 | tf_op jit(solution)/shard_map/all_to_all | solution.py:71
  17.7 20.5 %all-gather.2.cloned.1.call-start = ((), (), s32[]{:S(2)}) async-start(), calls=%async_computation.4 | async-start | bytes 1310720 | tf_op jit(solution)/shard_map/all_gather | solution.py:59
  83.7 80.6 %all-to-all-start.2 = ((bf16[128,8,1024]{0,2,1:T(8,128)(2,1)}), bf16[128,8,1024]{0,2,1:T(8,128)(2,1)}, u32[]{:S(2)}, u32[]{:S(2)}) async-start(bf16[128,8,1024]{0,2,1:T(8,128)(2,1)} %bitcast.10), calls=%async_computation.2 | async-start | bytes 4194304 | tf_op jit(solution)/shard_map/all_to_all | solution.py:72
  182.2 3.2 %copy-start = (f32[4,512,1024]{2,1,0:T(8,128)}, f32[4,512,1024]{2,1,0:T(8,128)S(1)}, u32[]{:S(2)}) copy-start(f32[4,512,1024]{2,1,0:T(8,128)S(1)} %fusion.52) | copy-start | bytes 25165828 | tf_op jit(solution)/shard_map/while/body/eval_jaxpr/while
  201.1 3.2 %copy-start = (f32[4,512,1024]{2,1,0:T(8,128)}, f32[4,512,1024]{2,1,0:T(8,128)S(1)}, u32[]{:S(2)}) copy-start(f32[4,512,1024]{2,1,0:T(8,128)S(1)} %fusion.52) | copy-start | bytes 25165828 | tf_op jit(solution)/shard_map/while/body/eval_jaxpr/while
  217.5 5.9 %copy-start.2 = (bf16[128,4096]{1,0:T(8,128)(2,1)S(1)}, bf16[128,4096]{1,0:T(8,128)(2,1)}, u32[]{:S(2)}) copy-start(bf16[128,4096]{1,0:T(8,128)(2,1)} %param.14) | copy-start | bytes 3145732
  219.8 25.3 %all-to-all-start.3 = ((bf16[8,128,512]{2,1,0:T(8,128)(2,1)}), bf16[8,128,512]{2,1,0:T(8,128)(2,1)S(1)}, u32[]{:S(2)}, u32[]{:S(2)}) async-start(bf16[8,128,512]{2,1,0:T(8,128)(2,1)} %all_to_all.55), calls=%async_computation.3 | async-start | bytes 2097152 | tf_op jit(solution)/shard_map/all_to_all | solution.py:99
  248.6 0.8 copy-start.3
Sparse Core Ops, SparseCore 0:
  20.0 18.0 all-gather.1
where the time goes:
time: 261 us; the launch traced here: 260 us
  blocking collectives  95.9 us (37%)
  waiting for transfers between devices  47.9 us (18%)
  local copies, waits for them, and re-layouts  43.7 us (17%)
  matrix products  33 us (13%)
  starting transfers between devices  15.4 us (6%)
  between operations  13.6 us (5%)
  other arithmetic  10.8 us (4%)
    all_gather x1, blocking collectives, per_device(): lax.all_gather(rotary(rope_key, position), 'sp', axis=0, tiled=True)  67 us
    all_to_all x1, blocking collectives, per_device(): lax.all_to_all(shard_columns, 'dp', split_axis=0, concat_axis=1, tiled=True)  28.9 us
    dot_general x2, matrix products, attend(): jnp.einsum('hqk,khd->qhd', weights, values, preferred_element_type=jnp.fl...  21.9 us
    all_to_all x1, waiting for transfers between devices, per_device(): lax.all_to_all(heads_out, 'sp', split_axis=0, concat_axis=1, tiled=True)  21 us
    all_gather x1, waiting for transfers between devices, per_device(): lax.all_gather(normed, 'dp', axis=0, tiled=True)  19.4 us
    while x3, local copies, waits for them, and re-layouts, one_sequence(): lax.map(lambda piece_rows: attend(piece_rows, keys_plain, rope_seq, value...  8.49 us
    all_to_all x1, starting transfers between devices, per_device(): lax.all_to_all(head_queries, 'sp', split_axis=1, concat_axis=0, tiled=True)  7.44 us
    all_to_all x1, waiting for transfers between devices, per_device(): lax.all_to_all(head_queries, 'sp', split_axis=1, concat_axis=0, tiled=True)  7.4 us
  transfers between devices with their start and end apart: 4, of which 3 were waited for; matrix products, arithmetic and copies ran while one was open for 8% of the time, Pallas kernels for 0%

commit v1 on v0

v1 whole, which is shorter than its diff:
```python
import functools

import jax
import jax.numpy as jnp
import numpy as np
from jax import lax
from jax.experimental import pallas as pl
from jax.experimental.pallas import tpu as pltpu
from jax.sharding import PartitionSpec as P

HEADS = 32
NOPE = 128
ROPE = 64
VDIM = 128
QDIM = NOPE + ROPE
KDIM = 256

EPS = 1e-06
THETA = 10000.0
LOG2E = 1.4426950408889634

MESH = pl.DeviceIdType.MESH
DN_T = (((1,), (1,)), ((), ()))


def turn(x, cosine, sine, mask):
    partner = jnp.where(mask, pltpu.roll(x, 96, 1), pltpu.roll(x, 32, 1))
    return x * cosine + partner * sine


def kernel(
    n_s, n_d,
    q_ref, lat_ref, rk_ref, lgain_ref, w_ref, gate_ref, ogain_ref, ta_ref, tb_ref,
    out_ref,
    w_v, gate_v, latb, rkb, qb, kbuf, vbuf, rq, ob, orecv,
    w_sem, gate_sem, lat_send, lat_recv, rk_send, rk_recv, relay_lat, relay_rk,
    q_send, q_recv, o_send, o_recv,
):
    s, d = lax.axis_index("sp"), lax.axis_index("dp")
    rows = lat_ref.shape[0]
    heads = HEADS // n_d
    qcols, ocols = heads * QDIM, heads * VDIM
    groups = n_s // n_d
    zh, m = s // n_d, s % n_d
    core = d % 2
    partner = d + 1 - 2 * core

    def send(src, dst, ssem, rsem, ts, td):
        same = (ts == s) & (td == d)

        @pl.when(jnp.logical_not(same))
        def _():
            pltpu.make_async_remote_copy(
                src, dst, ssem, rsem, device_id={"sp": ts, "dp": td}, device_id_type=MESH
            ).start()

        @pl.when(same)
        def _():
            pltpu.make_async_copy(src, dst, rsem).start()

    def sent(src, dst, ssem, rsem, ts, td):
        same = (ts == s) & (td == d)

        @pl.when(jnp.logical_not(same))
        def _():
            pltpu.make_async_remote_copy(
                src, dst, ssem, rsem, device_id={"sp": ts, "dp": td}, device_id_type=MESH
            ).wait_send()

    def arrived(dst, rsem):
        pltpu.make_async_copy(dst, dst, rsem).wait()

    latent_sends = []
    for k in range(groups):
        for pair in range(n_d // 2):
            i = k * (n_d // 2) + pair
            to = (k * n_d + d, 2 * pair + s % 2)
            latent_sends.append((lat_ref, latb.at[s], lat_send.at[i], lat_recv.at[s], *to))
            latent_sends.append((rk_ref, rkb.at[s], rk_send.at[i], rk_recv.at[s], *to))
    query_sends = [
        (
            q_ref.at[:, pl.ds(t * qcols, qcols)], qb.at[m], q_send.at[t], q_recv.at[m],
            zh * n_d + d, jnp.int32(t),
        )
        for t in range(n_d)
    ]
    w_copy = pltpu.make_async_copy(w_ref, w_v, w_sem)
    gate_copy = pltpu.make_async_copy(gate_ref, gate_v, gate_sem)

    for args in latent_sends + query_sends:
        send(*args)
    w_copy.start()
    gate_copy.start()
    w_copy.wait()

    lane = lax.broadcasted_iota(jnp.int32, (rows, 128), 1)
    low = lane < 64
    mask = (lane % 64) < 32
    sign = jnp.where(mask, -1.0, 1.0).astype(jnp.float32)

    def tables(block):
        ca, sa = ta_ref[0], ta_ref[1]
        cb, sb = tb_ref[0, block], tb_ref[1, block]
        return ca * cb - sa * sb, (sa * cb + ca * sb) * sign

    def key_step(i, carry):
        slot = lax.rem(s + i, n_s)
        at = pl.ds(pl.multiple_of(slot * rows, rows), rows)
        arrived(latb.at[slot], lat_recv.at[slot])
        arrived(rkb.at[slot], rk_recv.at[slot])

        @pl.when(slot % 2 == core)
        def _():
            for buf, ssem, rsem in ((latb, relay_lat, lat_recv), (rkb, relay_rk, rk_recv)):
                pltpu.make_async_remote_copy(
                    buf.at[slot], buf.at[slot], ssem.at[slot // 2], rsem.at[slot],
                    device_id={"sp": s, "dp": partner}, device_id_type=MESH,
                ).start()

        wide = latb[slot].astype(jnp.float32)
        scale = lax.rsqrt(jnp.mean(wide * wide, axis=-1, keepdims=True) + EPS)
        normed = (wide * scale * lgain_ref[...]).astype(jnp.bfloat16)
        cosine, sine = tables(slot)
        raw = rkb[slot].astype(jnp.float32)
        rot = turn(jnp.concatenate([raw, jnp.zeros_like(raw)], axis=1), cosine, sine, mask)
        rot_high = pltpu.roll(rot, 64, 1)
        for h in range(heads):
            both = jnp.dot(
                normed, w_v[:, h * 256 : (h + 1) * 256], preferred_element_type=jnp.float32
            )
            plain = both[:, :NOPE]
            if h % 2 == 0:
                first, second = plain, rot
            else:
                moved = pltpu.roll(plain, 64, 1)
                first = jnp.where(low, 0.0, moved)
                second = jnp.where(low, moved, rot_high)
            kbuf[h, at, :128] = first.astype(jnp.bfloat16)
            kbuf[h, at, 128:] = second.astype(jnp.bfloat16)
            vbuf[h, at, :VDIM] = both[:, NOPE:].astype(jnp.bfloat16)
            vbuf[h, at, VDIM:] = jnp.ones((rows, 128), jnp.bfloat16)
        return carry

    lax.fori_loop(0, n_s, key_step, 0)

    factor = LOG2E * QDIM ** -0.5

    def output_send(j):
        return (ob.at[j], orecv.at[d], o_send.at[j], o_recv.at[d], zh * n_d + j, m)

    def query_step(r, carry):
        for half in range(2):
            slot = 2 * r + half
            arrived(qb.at[slot], q_recv.at[slot])
            cosine, sine = tables(zh * n_d + slot)
            cosine_high, sine_high = pltpu.roll(cosine, 64, 1), pltpu.roll(sine, 64, 1)
            here = slice(half * rows, (half + 1) * rows)
            for p in range(heads // 2):
                c = p * 2 * QDIM
                rq[here, c : c + 128] = qb[slot, :, c : c + 128]
                x = qb[slot, :, c + 128 : c + 256].astype(jnp.float32)
                rq[here, c + 128 : c + 256] = turn(x, cosine, sine, mask).astype(jnp.bfloat16)
                x = qb[slot, :, c + 256 : c + 384].astype(jnp.float32)
                rq[here, c + 256 : c + 384] = turn(x, cosine_high, sine_high, mask).astype(jnp.bfloat16)

        def head_pair(p, carry):
            for odd in range(2):
                h = 2 * p + odd
                col = pl.multiple_of(p * (2 * QDIM) + odd * 128, 128)
                scores = lax.dot_general(
                    rq[:, pl.ds(col, KDIM)], kbuf[h], DN_T, preferred_element_type=jnp.float32
                )
                top = jnp.max(scores, axis=-1, keepdims=True)
                raised = jnp.exp2((scores - top) * factor).astype(jnp.bfloat16)
                total = jnp.dot(raised, vbuf[h], preferred_element_type=jnp.float32)
                result = (total[:, :VDIM] / total[:, VDIM:]).astype(jnp.bfloat16)
                at = pl.ds(pl.multiple_of(h * VDIM, VDIM), VDIM)
                ob[2 * r, :, at] = result[:rows]
                ob[2 * r + 1, :, at] = result[rows:]
            return carry

        lax.fori_loop(0, heads // 2, head_pair, 0)
        send(*output_send(2 * r))
        send(*output_send(2 * r + 1))
        return carry

    lax.fori_loop(0, n_d // 2, query_step, 0)

    gate_copy.wait()
    square = jnp.zeros((rows, 1), jnp.float32)
    for t in range(n_d):
        arrived(orecv.at[t], o_recv.at[t])
        g = gate_v[:, t * ocols : (t + 1) * ocols].astype(jnp.float32)
        gated = orecv[t].astype(jnp.float32) * (g / (1.0 + jnp.exp(-g)))
        square = square + jnp.sum(gated * gated, axis=-1, keepdims=True)
    scale = lax.rsqrt(square / (HEADS * VDIM) + EPS)
    for t in range(n_d):
        cols = slice(t * ocols, (t + 1) * ocols)
        g = gate_v[:, cols].astype(jnp.float32)
        gated = orecv[t].astype(jnp.float32) * (g / (1.0 + jnp.exp(-g)))
        out_ref[:, cols] = (gated * scale * ogain_ref[:, cols]).astype(jnp.bfloat16)

    for args in latent_sends + query_sends:
        sent(*args)
    for half in range(n_s // 2):
        slot = 2 * half + core
        for buf, ssem, rsem in ((latb, relay_lat, lat_recv), (rkb, relay_rk, rk_recv)):
            pltpu.make_async_remote_copy(
                buf.at[slot], buf.at[slot], ssem.at[half], rsem.at[slot],
                device_id={"sp": s, "dp": partner}, device_id_type=MESH,
            ).wait_send()
    for j in range(n_d):
        sent(*output_send(j))


def angle_tables(rows, n_s):
    half = ROPE // 2
    inverse = np.zeros(128)
    inverse[:ROPE] = np.tile(THETA ** (-np.arange(half) / half), 2)
    inner = np.arange(rows)[:, None] * inverse[None, :]
    outer = (np.arange(n_s) * rows)[:, None] * inverse[None, :]
    inner = np.stack([np.cos(inner), np.sin(inner)]).astype(np.float32)
    outer = np.stack([np.cos(outer), np.sin(outer)]).astype(np.float32)
    return jnp.asarray(inner), jnp.asarray(outer[:, :, None, :])


def per_device(n_s, n_d, queries, latent, rope_key, latent_gain, kv_weight, gate, out_gain):
    rows, rank = latent.shape
    heads = HEADS // n_d
    seq = rows * n_s
    inner, outer = angle_tables(rows, n_s)
    bf = jnp.bfloat16
    dma = pltpu.SemaphoreType.DMA
    vmem = pl.BlockSpec(memory_space=pltpu.VMEM)
    hbm = pl.BlockSpec(memory_space=pl.ANY)
    pieces = n_s // 2
    return pl.pallas_call(
        functools.partial(kernel, n_s, n_d),
        out_shape=jax.ShapeDtypeStruct(gate.shape, bf),
        in_specs=[hbm, vmem, vmem, vmem, hbm, hbm, vmem, vmem, vmem],
        out_specs=vmem,
        scratch_shapes=[
            pltpu.VMEM(kv_weight.shape, bf),
            pltpu.VMEM(gate.shape, bf),
            pltpu.VMEM((n_s, rows, rank), bf),
            pltpu.VMEM((n_s, rows, ROPE), bf),
            pltpu.VMEM((n_d, rows, heads * QDIM), bf),
            pltpu.VMEM((heads, seq, KDIM), bf),
            pltpu.VMEM((heads, seq, 2 * VDIM), bf),
            pltpu.VMEM((2 * rows, heads * QDIM), bf),
            pltpu.VMEM((n_d, rows, heads * VDIM), bf),
            pltpu.VMEM((n_d, rows, heads * VDIM), bf),
            dma, dma,
            dma((pieces,)), dma((n_s,)), dma((pieces,)), dma((n_s,)),
            dma((pieces,)), dma((pieces,)),
            dma((n_d,)), dma((n_d,)), dma((n_d,)), dma((n_d,)),
        ],
        compiler_params=pltpu.CompilerParams(
            has_side_effects=True, vmem_limit_bytes=60 * 1024 * 1024
        ),
        name="latent_attention",
    )(
        queries, latent, rope_key, latent_gain[None, :], kv_weight, gate, out_gain[None, :],
        inner, outer,
    )


def solution(mesh):
    return jax.shard_map(
        functools.partial(per_device, mesh.shape["sp"], mesh.shape["dp"]),
        mesh=mesh,
        in_specs=(
            P(("dp", "sp"), None),
            P(("dp", "sp"), None),
            P(("dp", "sp"), None),
            P(),
            P(None, "dp"),
            P(("dp", "sp"), None),
            P(),
        ),
        out_specs=P(("dp", "sp"), None),
        check_vma=False,
    )
```

time: 261 us -> 103 us (0.39)
  the two profiles are of different devices: /device:TPU:0 before, /device:TPU:12 now
where the time goes in v1:
time: 103 us
  Pallas kernels  99.4 us (97%)
  local copies, waits for them, and re-layouts  3.72 us (4%)
    pallas_call x1, Pallas kernels, per_device(): pl.pallas_call(functools.partial(kernel, n_s, n_d), out_shape=jax.ShapeDt...  99.4 us
    unnamed x2, local copies, waits for them, and re-layouts  3.72 us

profile of v1, /device:TPU:12, one launch (start us, length us, event | category | flops | bytes accessed | tf_op | source)
XLA Modules:
  0.0 103.1 jit_solution(14546992742916355651)
XLA Ops:
  0.0 1.4 %copy.10.rk_ref = bf16[128,64]{1,0:T(8,128)(2,1)} copy(bf16[128,64]{0,1:T(8,128)(2,1)} %param.11) | data formatting | bytes 32768 | tf_op args[2]
  1.4 99.4 %latent_attention.1 = bf16[128,4096]{1,0:T(8,128)(2,1)} custom-call(bf16[128,6144]{1,0:T(8,128)(2,1)} %q_ref.1, bf16[128,1024]{1,0:T(8,128)(2,1)} %lat_ref.1, bf16[128,64]{1,0:T(8,128)(2,1)} %copy.10.rk_ref, f32[1,1024]{1,0:T(1,128)} %bitcast.3, bf16[1024,2048]{1,0:T(8,128)(2,1)} %w_ref.1, bf16[128,4096]{1,0:T(8,128)(2,1)} %gate_ref.1, f32[1,4096]{1,0:T(1,128)} %bitcast.2, ...), custom_call_target="tpu_custom_call" | custom-call | tf_op jit(solution)/shard_map/latent_attention/pallas_call | solution.py:237
  100.8 2.3 %copy.12 = bf16[128,4096]{1,0:T(8,128)(2,1)} copy(bf16[128,4096]{1,0:T(8,128)(2,1)} %latent_attention.1) | data formatting | bytes 2097152

commit v2 on v1

--- a/solution.py
+++ b/solution.py
@@ -41,7 +41,10 @@
     heads = HEADS // n_d
     qcols, ocols = heads * QDIM, heads * VDIM
     groups = n_s // n_d
+    half = n_d // 2
     zh, m = s // n_d, s % n_d
+    seq = 2 * ((m % half - m // half + half) % half) + m // half
+    home = (d % 2) * half + (d // 2 + d % 2) % half
     core = d % 2
     partner = d + 1 - 2 * core
 
@@ -74,13 +77,13 @@
     for k in range(groups):
         for pair in range(n_d // 2):
             i = k * (n_d // 2) + pair
-            to = (k * n_d + d, 2 * pair + s % 2)
+            to = (k * n_d + home, 2 * pair + s % 2)
             latent_sends.append((lat_ref, latb.at[s], lat_send.at[i], lat_recv.at[s], *to))
             latent_sends.append((rk_ref, rkb.at[s], rk_send.at[i], rk_recv.at[s], *to))
     query_sends = [
         (
             q_ref.at[:, pl.ds(t * qcols, qcols)], qb.at[m], q_send.at[t], q_recv.at[m],
-            zh * n_d + d, jnp.int32(t),
+            zh * n_d + home, jnp.int32(t),
         )
         for t in range(n_d)
     ]
@@ -103,8 +106,17 @@
         cb, sb = tb_ref[0, block], tb_ref[1, block]
         return ca * cb - sa * sb, (sa * cb + ca * sb) * sign
 
+    def nearest(i):
+        if n_s & (n_s - 1):
+            return (s + i) % n_s
+        out, bit = 0, 1
+        while bit < n_s:
+            out = out + bit * ((s // bit + i // bit) % 2)
+            bit *= 2
+        return out
+
     def key_step(i, carry):
-        slot = lax.rem(s + i, n_s)
+        slot = nearest(i)
         at = pl.ds(pl.multiple_of(slot * rows, rows), rows)
         arrived(latb.at[slot], lat_recv.at[slot])
         arrived(rkb.at[slot], rk_recv.at[slot])
@@ -146,15 +158,16 @@
     factor = LOG2E * QDIM ** -0.5
 
     def output_send(j):
-        return (ob.at[j], orecv.at[d], o_send.at[j], o_recv.at[d], zh * n_d + j, m)
-
-    def query_step(r, carry):
-        for half in range(2):
-            slot = 2 * r + half
+        return (ob.at[j], orecv.at[d], o_send.at[j], o_recv.at[d], zh * n_d + j, seq)
+
+    def query_step(i, carry):
+        r = (i + m // 2) % half
+        for part in range(2):
+            slot = 2 * r + part
             arrived(qb.at[slot], q_recv.at[slot])
             cosine, sine = tables(zh * n_d + slot)
             cosine_high, sine_high = pltpu.roll(cosine, 64, 1), pltpu.roll(sine, 64, 1)
-            here = slice(half * rows, (half + 1) * rows)
+            here = slice(part * rows, (part + 1) * rows)
             for p in range(heads // 2):
                 c = p * 2 * QDIM
                 rq[here, c : c + 128] = qb[slot, :, c : c + 128]
@@ -184,7 +197,7 @@
         send(*output_send(2 * r + 1))
         return carry
 
-    lax.fori_loop(0, n_d // 2, query_step, 0)
+    lax.fori_loop(0, half, query_step, 0)
 
     gate_copy.wait()
     square = jnp.zeros((rows, 1), jnp.float32)
@@ -202,11 +215,11 @@
 
     for args in latent_sends + query_sends:
         sent(*args)
-    for half in range(n_s // 2):
-        slot = 2 * half + core
+    for part in range(n_s // 2):
+        slot = 2 * part + core
         for buf, ssem, rsem in ((latb, relay_lat, lat_recv), (rkb, relay_rk, rk_recv)):
             pltpu.make_async_remote_copy(
-                buf.at[slot], buf.at[slot], ssem.at[half], rsem.at[slot],
+                buf.at[slot], buf.at[slot], ssem.at[part], rsem.at[slot],
                 device_id={"sp": s, "dp": partner}, device_id_type=MESH,
             ).wait_send()
     for j in range(n_d):

time: 103 us -> 74.7 us (0.73)
  Pallas kernels: 99.4 us -> 70.8 us
    pallas_call x1, Pallas kernels: 99.4 us -> 70.8 us  [per_device(): pl.pallas_call(functools.partial(kernel, n_s, n_d), out_shape=jax.ShapeDt...]
where the time goes in v2:
time: 74.7 us; the launch traced here: 74.5 us
  Pallas kernels  70.8 us (95%)
  local copies, waits for them, and re-layouts  3.72 us (5%)
    pallas_call x1, Pallas kernels, per_device(): pl.pallas_call(functools.partial(kernel, n_s, n_d), out_shape=jax.ShapeDt...  70.8 us
    unnamed x2, local copies, waits for them, and re-layouts  3.72 us

profile of v2, /device:TPU:12, one launch (start us, length us, event | category | flops | bytes accessed | tf_op | source)
XLA Modules:
  0.0 74.5 jit_solution(6128177965921567548)
XLA Ops:
  0.0 1.4 %copy.10.rk_ref = bf16[128,64]{1,0:T(8,128)(2,1)} copy(bf16[128,64]{0,1:T(8,128)(2,1)} %param.11) | data formatting | bytes 32768 | tf_op args[2]
  1.4 70.8 %latent_attention.1 = bf16[128,4096]{1,0:T(8,128)(2,1)} custom-call(bf16[128,6144]{1,0:T(8,128)(2,1)} %q_ref.1, bf16[128,1024]{1,0:T(8,128)(2,1)} %lat_ref.1, bf16[128,64]{1,0:T(8,128)(2,1)} %copy.10.rk_ref, f32[1,1024]{1,0:T(1,128)} %bitcast.3, bf16[1024,2048]{1,0:T(8,128)(2,1)} %w_ref.1, bf16[128,4096]{1,0:T(8,128)(2,1)} %gate_ref.1, f32[1,4096]{1,0:T(1,128)} %bitcast.2, ...), custom_call_target="tpu_custom_call" | custom-call | tf_op jit(solution)/shard_map/latent_attention/pallas_call | solution.py:250
  72.2 2.3 %copy.12 = bf16[128,4096]{1,0:T(8,128)(2,1)} copy(bf16[128,4096]{1,0:T(8,128)(2,1)} %latent_attention.1) | data formatting | bytes 2097152

commit v3 on v2

--- a/solution.py
+++ b/solution.py
@@ -13,6 +13,7 @@
 ROPE = 64
 VDIM = 128
 QDIM = NOPE + ROPE
+PAIR = 2 * QDIM
 KDIM = 256
 
 EPS = 1e-06
@@ -39,7 +40,7 @@
     s, d = lax.axis_index("sp"), lax.axis_index("dp")
     rows = lat_ref.shape[0]
     heads = HEADS // n_d
-    qcols, ocols = heads * QDIM, heads * VDIM
+    pairs = heads // 2
     groups = n_s // n_d
     half = n_d // 2
     zh, m = s // n_d, s % n_d
@@ -82,9 +83,10 @@
             latent_sends.append((rk_ref, rkb.at[s], rk_send.at[i], rk_recv.at[s], *to))
     query_sends = [
         (
-            q_ref.at[:, pl.ds(t * qcols, qcols)], qb.at[m], q_send.at[t], q_recv.at[m],
-            zh * n_d + home, jnp.int32(t),
+            q_ref.at[:, pl.ds((t * pairs + p) * PAIR, PAIR)], qb.at[m, p],
+            q_send.at[t, p], q_recv.at[m, p], zh * n_d + home, jnp.int32(t),
         )
+        for p in range(pairs)
         for t in range(n_d)
     ]
     w_copy = pltpu.make_async_copy(w_ref, w_v, w_sem)
@@ -133,7 +135,7 @@
         scale = lax.rsqrt(jnp.mean(wide * wide, axis=-1, keepdims=True) + EPS)
         normed = (wide * scale * lgain_ref[...]).astype(jnp.bfloat16)
         cosine, sine = tables(slot)
-        raw = rkb[slot].astype(jnp.float32)
+        raw = rkb[slot].astype(jnp.float32).T
         rot = turn(jnp.concatenate([raw, jnp.zeros_like(raw)], axis=1), cosine, sine, mask)
         rot_high = pltpu.roll(rot, 64, 1)
         for h in range(heads):
@@ -157,61 +159,57 @@
 
     factor = LOG2E * QDIM ** -0.5
 
-    def output_send(j):
-        return (ob.at[j], orecv.at[d], o_send.at[j], o_recv.at[d], zh * n_d + j, seq)
+    def output_send(j, p):
+        return (ob.at[j, p], orecv.at[d, p], o_send.at[j, p], o_recv.at[d, p], zh * n_d + j, seq)
 
     def query_step(i, carry):
-        r = (i + m // 2) % half
+        r, p = (i // pairs + m // 2) % half, i % pairs
         for part in range(2):
             slot = 2 * r + part
-            arrived(qb.at[slot], q_recv.at[slot])
+            arrived(qb.at[slot, p], q_recv.at[slot, p])
             cosine, sine = tables(zh * n_d + slot)
             cosine_high, sine_high = pltpu.roll(cosine, 64, 1), pltpu.roll(sine, 64, 1)
             here = slice(part * rows, (part + 1) * rows)
-            for p in range(heads // 2):
-                c = p * 2 * QDIM
-                rq[here, c : c + 128] = qb[slot, :, c : c + 128]
-                x = qb[slot, :, c + 128 : c + 256].astype(jnp.float32)
-                rq[here, c + 128 : c + 256] = turn(x, cosine, sine, mask).astype(jnp.bfloat16)
-                x = qb[slot, :, c + 256 : c + 384].astype(jnp.float32)
-                rq[here, c + 256 : c + 384] = turn(x, cosine_high, sine_high, mask).astype(jnp.bfloat16)
-
-        def head_pair(p, carry):
-            for odd in range(2):
-                h = 2 * p + odd
-                col = pl.multiple_of(p * (2 * QDIM) + odd * 128, 128)
-                scores = lax.dot_general(
-                    rq[:, pl.ds(col, KDIM)], kbuf[h], DN_T, preferred_element_type=jnp.float32
-                )
-                top = jnp.max(scores, axis=-1, keepdims=True)
-                raised = jnp.exp2((scores - top) * factor).astype(jnp.bfloat16)
-                total = jnp.dot(raised, vbuf[h], preferred_element_type=jnp.float32)
-                result = (total[:, :VDIM] / total[:, VDIM:]).astype(jnp.bfloat16)
-                at = pl.ds(pl.multiple_of(h * VDIM, VDIM), VDIM)
-                ob[2 * r, :, at] = result[:rows]
-                ob[2 * r + 1, :, at] = result[rows:]
-            return carry
-
-        lax.fori_loop(0, heads // 2, head_pair, 0)
-        send(*output_send(2 * r))
-        send(*output_send(2 * r + 1))
+            rq[here, :128] = qb[slot, p, :, :128]
+            x = qb[slot, p, :, 128:256].astype(jnp.float32)
+            rq[here, 128:256] = turn(x, cosine, sine, mask).astype(jnp.bfloat16)
+            x = qb[slot, p, :, 256:].astype(jnp.float32)
+            rq[here, 256:] = turn(x, cosine_high, sine_high, mask).astype(jnp.bfloat16)
+        for odd in range(2):
+            h = 2 * p + odd
+            scores = lax.dot_general(
+                rq[:, odd * 128 : odd * 128 + KDIM], kbuf[h], DN_T, preferred_element_type=jnp.float32
+            )
+            top = jnp.max(scores, axis=-1, keepdims=True)
+            raised = jnp.exp2((scores - top) * factor).astype(jnp.bfloat16)
+            total = jnp.dot(raised, vbuf[h], preferred_element_type=jnp.float32)
+            result = (total[:, :VDIM] / total[:, VDIM:]).astype(jnp.bfloat16)
+            at = slice(odd * VDIM, (odd + 1) * VDIM)
+            ob[2 * r, p, :, at] = result[:rows]
+            ob[2 * r + 1, p, :, at] = result[rows:]
+        send(*output_send(2 * r, p))
+        send(*output_send(2 * r + 1, p))
         return carry
 
-    lax.fori_loop(0, half, query_step, 0)
+    lax.fori_loop(0, half * pairs, query_step, 0)
 
     gate_copy.wait()
+    def gated_piece(t, p):
+        c = (t * pairs + p) * 2 * VDIM
+        g = gate_v[:, c : c + 2 * VDIM].astype(jnp.float32)
+        return slice(c, c + 2 * VDIM), orecv[t, p].astype(jnp.float32) * (g / (1.0 + jnp.exp(-g)))
+
     square = jnp.zeros((rows, 1), jnp.float32)
-    for t in range(n_d):
-        arrived(orecv.at[t], o_recv.at[t])
-        g = gate_v[:, t * ocols : (t + 1) * ocols].astype(jnp.float32)
-        gated = orecv[t].astype(jnp.float32) * (g / (1.0 + jnp.exp(-g)))
-        square = square + jnp.sum(gated * gated, axis=-1, keepdims=True)
+    for p in range(pairs):
+        for t in range(n_d):
+            arrived(orecv.at[t, p], o_recv.at[t, p])
+            _, gated = gated_piece(t, p)
+            square = square + jnp.sum(gated * gated, axis=-1, keepdims=True)
     scale = lax.rsqrt(square / (HEADS * VDIM) + EPS)
     for t in range(n_d):
-        cols = slice(t * ocols, (t + 1) * ocols)
-        g = gate_v[:, cols].astype(jnp.float32)
-        gated = orecv[t].astype(jnp.float32) * (g / (1.0 + jnp.exp(-g)))
-        out_ref[:, cols] = (gated * scale * ogain_ref[:, cols]).astype(jnp.bfloat16)
+        for p in range(pairs):
+            cols, gated = gated_piece(t, p)
+            out_ref[:, cols] = (gated * scale * ogain_ref[:, cols]).astype(jnp.bfloat16)
 
     for args in latent_sends + query_sends:
         sent(*args)
@@ -222,8 +220,12 @@
                 buf.at[slot], buf.at[slot], ssem.at[part], rsem.at[slot],
                 device_id={"sp": s, "dp": partner}, device_id_type=MESH,
             ).wait_send()
-    for j in range(n_d):
-        sent(*output_send(j))
+
+    def output_sent(i, carry):
+        sent(*output_send(i // pairs, i % pairs))
+        return carry
+
+    lax.fori_loop(0, n_d * pairs, output_sent, 0)
 
 
 def angle_tables(rows, n_s):
@@ -240,6 +242,7 @@
 def per_device(n_s, n_d, queries, latent, rope_key, latent_gain, kv_weight, gate, out_gain):
     rows, rank = latent.shape
     heads = HEADS // n_d
+    pairs = heads // 2
     seq = rows * n_s
     inner, outer = angle_tables(rows, n_s)
     bf = jnp.bfloat16
@@ -256,24 +259,24 @@
             pltpu.VMEM(kv_weight.shape, bf),
             pltpu.VMEM(gate.shape, bf),
             pltpu.VMEM((n_s, rows, rank), bf),
-            pltpu.VMEM((n_s, rows, ROPE), bf),
-            pltpu.VMEM((n_d, rows, heads * QDIM), bf),
+            pltpu.VMEM((n_s, ROPE, rows), bf),
+            pltpu.VMEM((n_d, pairs, rows, PAIR), bf),
             pltpu.VMEM((heads, seq, KDIM), bf),
             pltpu.VMEM((heads, seq, 2 * VDIM), bf),
-            pltpu.VMEM((2 * rows, heads * QDIM), bf),
-            pltpu.VMEM((n_d, rows, heads * VDIM), bf),
-            pltpu.VMEM((n_d, rows, heads * VDIM), bf),
+            pltpu.VMEM((2 * rows, PAIR), bf),
+            pltpu.VMEM((n_d, pairs, rows, 2 * VDIM), bf),
+            pltpu.VMEM((n_d, pairs, rows, 2 * VDIM), bf),
             dma, dma,
             dma((pieces,)), dma((n_s,)), dma((pieces,)), dma((n_s,)),
             dma((pieces,)), dma((pieces,)),
-            dma((n_d,)), dma((n_d,)), dma((n_d,)), dma((n_d,)),
+            *[dma((n_d, pairs))] * 4,
         ],
         compiler_params=pltpu.CompilerParams(
             has_side_effects=True, vmem_limit_bytes=60 * 1024 * 1024
         ),
         name="latent_attention",
     )(
-        queries, latent, rope_key, latent_gain[None, :], kv_weight, gate, out_gain[None, :],
+        queries, latent, rope_key.T, latent_gain[None, :], kv_weight, gate, out_gain[None, :],
         inner, outer,
     )
 

time: 74.7 us -> 67.9 us (0.909)
  Pallas kernels: 70.8 us -> 65.4 us
  local copies, waits for them, and re-layouts: 3.72 us -> 2.29 us
    pallas_call x1, Pallas kernels: 70.8 us -> 65.4 us  [per_device(): pl.pallas_call(functools.partial(kernel, n_s, n_d), out_shape=jax.ShapeDt...]
    unnamed x2 -> x1, local copies, waits for them, and re-layouts: 3.72 us -> 2.29 us
where the time goes in v3:
time: 67.9 us; the launch traced here: 67.7 us
  Pallas kernels  65.4 us (96%)
  local copies, waits for them, and re-layouts  2.29 us (3%)
    pallas_call x1, Pallas kernels, per_device(): pl.pallas_call(functools.partial(kernel, n_s, n_d), out_shape=jax.ShapeDt...  65.4 us
    unnamed x1, local copies, waits for them, and re-layouts  2.29 us

profile of v3, /device:TPU:12, one launch (start us, length us, event | category | flops | bytes accessed | tf_op | source)
XLA Modules:
  0.0 67.7 jit_solution(16665935661420270580)
XLA Ops:
  0.0 65.4 %latent_attention.1 = bf16[128,4096]{1,0:T(8,128)(2,1)} custom-call(bf16[128,6144]{1,0:T(8,128)(2,1)} %q_ref.1, bf16[128,1024]{1,0:T(8,128)(2,1)} %lat_ref.1, bf16[64,128]{1,0:T(8,128)(2,1)} %bitcast.3, f32[1,1024]{1,0:T(1,128)} %bitcast.5, bf16[1024,2048]{1,0:T(8,128)(2,1)} %w_ref.1, bf16[128,4096]{1,0:T(8,128)(2,1)} %gate_ref.1, f32[1,4096]{1,0:T(1,128)} %bitcast.4, ...), custom_call_target="tpu_custom_call" | custom-call | tf_op jit(solution)/shard_map/latent_attention/pallas_call | solution.py:253
  65.4 2.3 %copy.11 = bf16[128,4096]{1,0:T(8,128)(2,1)} copy(bf16[128,4096]{1,0:T(8,128)(2,1)} %latent_attention.1) | data formatting | bytes 2097152
